TPU v7x, 32 devices: a whole 2x2x4 slice. The times are simulated.
32 devices in a mesh: sp: 4 (over z), fs: 4 (over y, x), tp: 2 (over core).
Axes of the slice: x: 2, y: 2, z: 4, core: 2. Of those that a mesh axis runs over, the one named last changes fastest.
Arguments:
- tokens: bfloat16 [4, 1024, 2048], P('fs', 'sp', 'tp'), may hold values from -6 to 6
- norm_gain: float32 [2048], replicated, may hold values from 0.1 to 1.9
- ret_query: bfloat16 [2048, 1024], P('sp', 'tp'), may hold values from -0.125 to 0.125
- ret_key: bfloat16 [2048, 1024], P('sp', 'tp'), may hold values from -0.125 to 0.125
- ret_value: bfloat16 [2048, 1024], P('sp', 'tp'), may hold values from -0.125 to 0.125
- att_query: bfloat16 [2048, 1024], P('sp', 'tp'), may hold values from -0.125 to 0.125
- att_key: bfloat16 [2048, 256], P('sp', 'tp'), may hold values from -0.125 to 0.125
- att_value: bfloat16 [2048, 256], P('sp', 'tp'), may hold values from -0.125 to 0.125
- log_decay: float32 [4, 4, 1024], P('fs', 'tp', 'sp'), may hold values from -1 to 0
- start_state: float32 [4, 4, 256, 256], P('fs', 'tp'), may hold values from -12 to 12
- ret_gain: float32 [1024], P('tp'), may hold values from 0.1 to 1.9
- sink_logits: float32 [16], P('tp'), may hold values from 1 to 5
- ret_out: bfloat16 [1024, 2048], P('tp', 'fs'), may hold values from -0.1875 to 0.1875
- att_out: bfloat16 [1024, 2048], P('tp', 'fs'), may hold values from -1.5 to 1.5
Outputs:
- mixed: bfloat16 [4, 1024, 2048], P('fs', 'sp', 'tp')
All inputs are finite; a program needn't handle non-finite values.
Results may differ from a plain program's by a relative error of at most 0.015.
Values may be sent and summed in bfloat16 or wider, within the bound.
A program may use at most 128 MiB of HBM per device.

v0:
```python
import jax
import jax.numpy as jnp
from jax import lax
from jax.sharding import PartitionSpec as P

DK = 256
DV = 256
HD = 64
WINDOW = 128
BLOCK = 128
epsilon = 1e-06
exact_result = lax.Precision.HIGHEST


def carried_in(array, axis, combine, identity):
    peers, mine = (lax.axis_size(axis), lax.axis_index(axis))
    everything = jax.tree.map(
        lambda part, kind: lax.all_gather(part.astype(kind), axis),
        array,
        (jnp.bfloat16, jnp.bfloat16),
    )
    start = jax.tree.map(
        lambda part, zero: jnp.broadcast_to(jnp.asarray(zero, part.dtype), part.shape),
        array,
        identity,
    )

    def hop(k, before):
        reached = k < mine
        new = combine(
            before, jax.tree.map(lambda part, own: part[k].astype(own.dtype), everything, array)
        )
        return jax.tree.map(lambda a, b: jnp.where(reached, a, b), new, before)

    return lax.fori_loop(0, peers, hop, start)


def passed_along(block, axis, distance):
    devices = range(lax.axis_size(axis))
    route = [(i - distance, i) for i in devices if i - distance in devices]
    return lax.ppermute(block, axis, route)


def rotate(values, positions):
    half_dim = values.shape[-1] // 2
    inverse = 1.0 / 10000.0 ** (jnp.arange(half_dim, dtype=jnp.float32) / half_dim)
    angles = positions.astype(jnp.float32)[:, None] * inverse[None, :]
    cosine = jnp.cos(angles)[:, None, :]
    sine_table = jnp.sin(angles)[:, None, :]
    front_half = values[..., :half_dim]
    back_half = values[..., half_dim:]
    return jnp.concatenate(
        [
            front_half * cosine - back_half * sine_table,
            front_half * sine_table + back_half * cosine,
        ],
        axis=-1,
    )


def block_step(memory_state, inputs):
    queries, key_matrix_rows, value_matrix_rows, log_rates = inputs
    length_here = log_rates.shape[-1]
    causal = jnp.arange(length_here)[:, None] >= jnp.arange(length_here)[None, :]
    running_totals = jnp.cumsum(log_rates, axis=-1)
    relative = running_totals[:, :, None] - running_totals[:, None, :]
    weight = jnp.where(causal[None], jnp.exp(jnp.where(causal[None], relative, 0.0)), 0.0)
    score_matrix = (
        jnp.einsum("hqd,hkd->hqk", queries, key_matrix_rows, precision=exact_result) * weight
    )
    carried_state = jnp.einsum(
        "hqd,hdv->hqv",
        queries * jnp.exp(running_totals)[:, :, None],
        memory_state,
        precision=exact_result,
    )
    output_rows = (
        jnp.einsum("arf,afu->aru", score_matrix, value_matrix_rows, precision=exact_result)
        + carried_state
    )
    decay_factors = jnp.exp(running_totals[:, -1:] - running_totals)
    memory_state = memory_state * jnp.exp(running_totals[:, -1])[:, None, None] + jnp.einsum(
        "iwj,iwe->ije",
        key_matrix_rows * decay_factors[:, :, None],
        value_matrix_rows,
        precision=exact_result,
    )
    return (memory_state, output_rows)


def chain(earlier, later):
    return (earlier[0] * later[0], earlier[1] * later[0][:, None, None] + later[1])


def shards(
    tokens,
    norm_gain,
    ret_query,
    ret_key,
    ret_value,
    att_query,
    att_key,
    att_value,
    log_decay,
    start_state,
    ret_gain,
    sink_logits,
    ret_out,
    att_out,
):
    gathered = lax.all_gather(tokens[0], "tp", axis=1, tiled=True)
    row_count = gathered.shape[0]
    as_float = gathered.astype(jnp.float32)
    normed = (
        as_float
        * lax.rsqrt(jnp.mean(as_float * as_float, axis=-1, keepdims=True) + epsilon)
        * norm_gain
    ).astype(jnp.bfloat16)
    offset = lax.axis_index("sp") * row_count
    positions = offset + jnp.arange(row_count, dtype=jnp.int32)
    weights = (ret_query, ret_key, ret_value, att_query, att_key, att_value)
    pieces = (
        lax.all_gather(weights[0], "sp", axis=0, tiled=True),
        lax.all_gather(weights[1], "sp", axis=0, tiled=True),
        lax.all_gather(weights[2], "sp", axis=0, tiled=True),
        lax.all_gather(weights[3], "sp", axis=0, tiled=True),
        lax.all_gather(weights[4], "sp", axis=0, tiled=True),
        lax.all_gather(weights[5], "sp", axis=0, tiled=True),
    )
    projected = tuple(
        (jnp.dot(normed, piece, preferred_element_type=jnp.float32) for piece in pieces)
    )
    rounded = tuple((product_f.astype(jnp.bfloat16) for product_f in projected))
    projected = rounded[:3]
    head_count = projected[0].shape[1] // DK
    queries = rotate(projected[0].astype(jnp.float32).reshape(row_count, head_count, DK), positions)
    keys_rot = rotate(
        projected[1].astype(jnp.float32).reshape(row_count, head_count, DK), positions
    ) * DK ** (-0.5)
    values_f = projected[2].astype(jnp.float32).reshape(row_count, head_count, DV)
    log_rates = log_decay[0]
    count = row_count // BLOCK

    def blocked(array):
        return array.reshape(count, BLOCK, head_count, array.shape[-1]).transpose(0, 2, 1, 3)

    rates_blocked = log_rates.reshape(head_count, count, BLOCK).transpose(1, 0, 2)
    local_state, pieces = lax.scan(
        block_step,
        jnp.zeros((head_count, DK, DV), jnp.float32),
        (blocked(queries), blocked(keys_rot), blocked(values_f), rates_blocked),
    )
    local_out = pieces.transpose(0, 2, 1, 3).reshape(row_count, head_count, DV)
    running_totals = jnp.cumsum(log_rates, axis=-1)
    device_decay = jnp.exp(running_totals[:, -1])
    identity = (jnp.ones((head_count,), jnp.float32), jnp.zeros((head_count, DK, DV), jnp.float32))
    prior_decay, prior_state = carried_in((device_decay, local_state), "sp", chain, identity)
    incoming = prior_state + prior_decay[:, None, None] * start_state[0]
    retained = local_out + jnp.einsum(
        "thd,hdv->thv",
        queries * jnp.exp(running_totals).T[:, :, None],
        incoming,
        precision=exact_result,
    )
    centred = retained - jnp.mean(retained, axis=-1, keepdims=True)
    variance = jnp.mean(centred * centred, axis=-1, keepdims=True)
    ret_hidden = (
        (centred * lax.rsqrt(variance + epsilon)).reshape(row_count, head_count * DV) * ret_gain
    ).astype(jnp.bfloat16)
    att_queries, att_keys, att_values = rounded[3:]
    kv_heads = att_keys.shape[1] // HD
    groups = att_queries.shape[1] // HD // kv_heads
    earlier_keys, earlier_values = passed_along(
        (att_keys[row_count - WINDOW :], att_values[row_count - WINDOW :]), "sp", 1
    )
    extended_keys = jnp.concatenate([earlier_keys, att_keys], axis=0)
    extended_values = jnp.concatenate([earlier_values, att_values], axis=0)
    windows = row_count // WINDOW

    def banded(array):
        earlier = array[:row_count].reshape(windows, WINDOW, kv_heads, HD)
        current = array[WINDOW:].reshape(windows, WINDOW, kv_heads, HD)
        return jnp.concatenate([earlier, current], axis=1)

    key_band = banded(extended_keys)
    value_band = banded(extended_values)
    grouped_q = att_queries.reshape(windows, WINDOW, kv_heads, groups, HD)
    score_matrix = jnp.einsum(
        "nqhgd,nkhd->nhgqk", grouped_q, key_band, preferred_element_type=jnp.float32
    ) * HD ** (-0.5)
    query_index = WINDOW + jnp.arange(WINDOW)
    key_index = jnp.arange(2 * WINDOW)
    allowed = (key_index[None, :] <= query_index[:, None]) & (
        query_index[:, None] - key_index[None, :] < WINDOW
    )
    key_place = offset - WINDOW + jnp.arange(windows)[:, None] * WINDOW + key_index[None, :]
    visible = (allowed[None] & (key_place >= 0)[:, None, :])[:, None, None]
    expo = jnp.exp(jnp.where(visible, score_matrix, -1e30))
    summed = jnp.sum(expo, axis=-1, keepdims=True) + jnp.exp(sink_logits).reshape(
        1, kv_heads, groups, 1, 1
    )
    probs = (expo / summed).astype(jnp.bfloat16)
    attended = jnp.einsum(
        "nhgqk,nkhd->nqhgd", probs, value_band, preferred_element_type=jnp.float32
    )
    att_hidden = attended.astype(jnp.bfloat16).reshape(row_count, kv_heads * groups * HD)
    ret_width = ret_hidden.shape[1]
    joined = jnp.concatenate([ret_hidden, att_hidden], axis=1)[None]
    piece = lax.all_gather(joined, "fs", axis=0, tiled=True)
    product = jnp.einsum(
        "srh,hd->srd", piece[:, :, :ret_width], ret_out, preferred_element_type=jnp.float32
    )
    product = product + jnp.einsum(
        "srh,hd->srd", piece[:, :, ret_width:], att_out, preferred_element_type=jnp.float32
    )
    partial_rows = product.astype(jnp.bfloat16)
    regrouped = lax.all_to_all(partial_rows, "fs", split_axis=0, concat_axis=2, tiled=True)
    mixed = lax.psum_scatter(
        regrouped[0].astype(jnp.float32).astype(jnp.bfloat16), "tp", scatter_dimension=1, tiled=True
    )
    return mixed[None]


def solution(mesh):
    placed = (
        P("fs", "sp", "tp"),
        P(),
        P("sp", "tp"),
        P("sp", "tp"),
        P("sp", "tp"),
        P("sp", "tp"),
        P("sp", "tp"),
        P("sp", "tp"),
        P("fs", "tp", "sp"),
        P("fs", "tp", None, None),
        P("tp"),
        P("tp"),
        P("tp", "fs"),
        P("tp", "fs"),
    )
    return jax.shard_map(
        shards, mesh=mesh, in_specs=placed, out_specs=P("fs", "sp", "tp"), check_vma=False
    )
```

profile of v0, /device:TPU:0, one launch (start us, length us, event | category | flops | bytes accessed | tf_op | source)
XLA Modules:
  0.0 330.0 jit_solution(6295431087866726067)
XLA Ops:
  13.0 13.6 %all-reduce = bf16[8]{0:T(256)(128)(2,1)S(1)} all-reduce(bf16[8]{0:T(256)(128)(2,1)S(1)} %dynamic-update-slice), channel_id=3, replica_groups=mesh['sp'=4,'fs'=4,'tp'=2] {'sp'}, use_global_device_ids=true, to_apply=%add | all-reduce | flops 8 | bytes 32
  26.6 18.4 %all_gather.42 = bf16[2048,128]{1,0:T(8,128)(2,1)S(1)} all-gather(bf16[512,128]{1,0:T(8,128)(2,1)S(1)} %copy-done.12), channel_id=1, replica_groups=mesh['sp'=4,'fs'=4,'tp'=2] {'sp'}, dimensions={0}, use_global_device_ids=true | all-gather | bytes 655360 | tf_op jit(solution)/shard_map/all_gather | solution.py:127
  45.7 21.2 %all_gather.41 = bf16[2048,128]{1,0:T(8,128)(2,1)} all-gather(bf16[512,128]{1,0:T(8,128)(2,1)S(1)} %copy-done.13), channel_id=1, replica_groups=mesh['sp'=4,'fs'=4,'tp'=2] {'sp'}, dimensions={0}, use_global_device_ids=true | all-gather | bytes 655360 | tf_op jit(solution)/shard_map/all_gather | solution.py:128
  66.9 1.2 multiply_cosine_fusion
  68.9 1.6 fusion.25
  70.5 1.7 convolution_convert_fusion.5
  72.9 2.6 collective-permute-start.1
  75.5 5.5 %all-gather.12.cloned.1.call-done = bf16[2048,512]{1,0:T(8,128)(2,1)} async-done(((bf16[512,512]{1,0:T(8,128)(2,1)}), bf16[2048,512]{1,0:T(8,128)(2,1)}) %all-gather.12.cloned.1.call-update) | async-done | bytes 2097168 | tf_op jit(solution)/shard_map/all_gather | solution.py:124
  80.9 2.3 fusion.31
  83.6 44.0 %all-gather.16.cloned.1.call-done = bf16[2048,512]{1,0:T(8,128)(2,1)} async-done(((bf16[512,512]{1,0:T(8,128)(2,1)}), bf16[2048,512]{1,0:T(8,128)(2,1)}) %all-gather.16.cloned.1.call-update) | async-done | bytes 2097168 | tf_op jit(solution)/shard_map/all_gather | solution.py:123
  127.6 2.7 fusion.33
  131.4 42.1 %all-gather.14.cloned.1.call-done = bf16[2048,512]{1,0:T(8,128)(2,1)} async-done(((bf16[512,512]{1,0:T(8,128)(2,1)}), bf16[2048,512]{1,0:T(8,128)(2,1)}) %all-gather.14.cloned.1.call-update) | async-done | bytes 2097168 | tf_op jit(solution)/shard_map/all_gather | solution.py:125
  173.6 2.7 fusion.32
  176.6 1.3 fusion.65
  178.9 6.7 %while.29 = (s32[]{:T(128)}, f32[2,256,256]{2,1,0:T(8,128)S(1)}, f32[2,2,128,256]{3,2,1,0:T(8,128)}, f32[2,2,128]{2,1,0:T(2,128)S(1)}, f32[2,2,128,256]{3,2,0,1:...) while((s32[]{:T(128)}, f32[2,256,256]{2,1,0:T(8,128)S(1)}, ...), condition=%wide.region_3.4_spmd.clone, body=%wide.region_1.3_spmd.clone.sunk | while | flops 604880896 | bytes 4242084 | solution.py:148
  180.2 1.2 fusion.95
  183.6 1.2 fusion.95
  186.4 1.9 convolution_convert_fusion.6
  188.6 2.3 collective-permute-start
  193.2 1.3 copy.65
  194.9 24.5 %all-gather.18.cloned.1.call-done = bf16[2048,512]{1,0:T(8,128)(2,1)} async-done(((bf16[512,512]{1,0:T(8,128)(2,1)}), bf16[2048,512]{1,0:T(8,128)(2,1)}) %all-gather.18.cloned.1.call-update) | async-done | bytes 2097168 | tf_op jit(solution)/shard_map/all_gather | solution.py:126
  219.5 2.3 convolution_convert_fusion.1
  223.8 25.1 %all-gather.22.cloned.1.call-done = bf16[8,256,256]{2,1,0:T(8,128)(2,1)} async-done(((bf16[2,256,256]{2,1,0:T(8,128)(2,1)}), bf16[8,256,256]{2,1,0:T(8,128)(2,1)}) %all-gather.22.cloned.1.call-update) | async-done | bytes 1048592 | tf_op jit(solution)/shard_map/all_gather | solution.py:18
  248.9 4.6 %while.30 = (s32[]{:T(128)}, f32[2]{0:T(128)S(1)}, f32[2,256,256]{2,1,0:T(8,128)S(1)}, s32[]{:T(128)}, bf16[4,2]{1,0:T(4,128)(2,1)S(1)}, /*index=5*/bf16[4,2,256,256]{3,2,1,0:T(8,128)(2,1)}, s32[]{:T(128)}, s32[]{:T(128)}) while((s32[]{:T(128)}, f32[2]{0:T(128)S(1)}, f32[2,256,256]{2,1,0:T(8,128)S(1)}, s32[]{:T(128)}, ...), condition=%wide.region_7.8_spmd.clone, body=%wide.region_6.7_spmd.clone.sunk | while | flops 655372 | bytes 1310871 | solution.py:35
  248.9 1.2 fusion.96
  253.6 1.2 fusion.67
  255.9 34.5 %all-gather.24.cloned.1.call-done = bf16[1024,1024]{0,1:T(8,128)(2,1)} async-done(((bf16[256,1024]{0,1:T(8,128)(2,1)}), bf16[1024,1024]{0,1:T(8,128)(2,1)}) %all-gather.24.cloned.1.call-update) | async-done | bytes 2097168 | tf_op jit(solution)/shard_map/all_gather | solution.py:209
  290.4 2.9 copy.81
  295.1 16.7 %all_to_all.15 = bf16[4,256,512]{2,1,0:T(8,128)(2,1)S(1)} all-to-all(bf16[4,256,512]{2,1,0:T(8,128)(2,1)S(1)} %add_convert_fusion), channel_id=1, replica_groups=mesh['sp'=4,'fs'=4,'tp'=2] {'fs'}, dimensions={0} | all-to-all | bytes 2097152 | tf_op jit(solution)/shard_map/all_to_all | solution.py:217
  311.8 1.3 copy.82
  313.1 8.0 %reduce-scatter.2.cloned.1.call-done = bf16[256,1024]{0,1:T(8,128)(2,1)} async-done(((bf16[256,2048]{0,1:T(8,128)(2,1)}), bf16[256,1024]{0,1:T(8,128)(2,1)}) %reduce-scatter.2.cloned.1.call-update) | async-done | bytes 524304 | tf_op jit(solution)/shard_map/reduce_scatter | solution.py:218
  321.1 2.0 copy.83
  (154 shorter events, 26.8 us)
Async XLA Ops:
  6.5 286.8 %copy-start = (bf16[512,512]{1,0:T(8,128)(2,1)S(1)}, bf16[512,512]{1,0:T(8,128)(2,1)}, u32[]{:S(2)}) copy-start(bf16[512,512]{1,0:T(8,128)(2,1)} %param.30) | copy-start | bytes 1572868
  6.5 4.8 %copy-start.23 = (u32[32]{0:T(128)S(1)}, u32[32]{0:T(128)}, u32[]{:S(2)}) copy-start(u32[32]{0:T(128)} %constant.93) | copy-start | bytes 388
  6.5 3.5 %copy-start.15 = (f32[1,2,256]{2,1,0:T(2,128)S(1)}, f32[1,2,256]{2,1,0:T(2,128)}, u32[]{:S(2)}) copy-start(f32[1,2,256]{2,1,0:T(2,128)} %param.26) | copy-start | bytes 6148
  6.5 20.1 %copy-start.12 = (bf16[512,128]{1,0:T(8,128)(2,1)S(1)}, bf16[512,128]{1,0:T(8,128)(2,1)}, u32[]{:S(2)}) copy-start(bf16[512,128]{1,0:T(8,128)(2,1)} %param.24) | copy-start | bytes 393220
  6.5 38.6 %copy-start.22 = (f32[8]{0:T(128)S(1)}, f32[8]{0:T(128)}, u32[]{:S(2)}) copy-start(f32[8]{0:T(128)} %param.29) | copy-start | bytes 100
  6.5 39.2 %copy-start.13 = (bf16[512,128]{1,0:T(8,128)(2,1)S(1)}, bf16[512,128]{1,0:T(8,128)(2,1)}, u32[]{:S(2)}) copy-start(bf16[512,128]{1,0:T(8,128)(2,1)} %param.25) | copy-start | bytes 393220
  6.6 62.3 %all-gather.20.cloned.1.call-start = ((), (), s32[]{:S(2)}) async-start(), calls=%async_computation.7 | async-start | bytes 1572864 | tf_op jit(solution)/shard_map/all_gather | solution.py:111
  7.3 73.6 %all-gather.12.cloned.1.call-start = ((), (), s32[]{:S(2)}) async-start(), calls=%async_computation.2 | async-start | bytes 2621440 | tf_op jit(solution)/shard_map/all_gather | solution.py:124
  8.0 62.5 %copy-start.20 = (f32[2048]{0:T(1024)S(1)}, f32[2048]{0:T(1024)}, u32[]{:S(2)}) copy-start(f32[2048]{0:T(1024)} %param.19) | copy-start | bytes 24580
  8.1 119.6 %all-gather.16.cloned.1.call-start = ((), (), s32[]{:S(2)}) async-start(), calls=%async_computation.4 | async-start | bytes 2621440 | tf_op jit(solution)/shard_map/all_gather | solution.py:123
  8.8 164.8 %all-gather.14.cloned.1.call-start = ((), (), s32[]{:S(2)}) async-start(), calls=%async_computation.3 | async-start | bytes 2621440 | tf_op jit(solution)/shard_map/all_gather | solution.py:125
  9.4 210.1 %all-gather.18.cloned.1.call-start = ((), (), s32[]{:S(2)}) async-start(), calls=%async_computation.5 | async-start | bytes 2621440 | tf_op jit(solution)/shard_map/all_gather | solution.py:126
  10.0 238.9 %all-gather.22.cloned.1.call-start = ((), (), s32[]{:S(2)}) async-start(), calls=%async_computation.8 | async-start | bytes 1310720 | tf_op jit(solution)/shard_map/all_gather | solution.py:18
  68.9 12.1 %copy-start.5 = (bf16[1,256,2048]{2,1,0:T(8,128)(2,1)S(1)}, bf16[1,256,2048]{2,1,0:T(8,128)(2,1)}, u32[]{:S(2)}) copy-start(bf16[1,256,2048]{2,1,0:T(8,128)(2,1)} %all-gather.20.cloned.1.call-done) | copy-start | bytes 3145732
  70.5 103.1 %copy-start.18 = (f32[256]{0:T(256)}, f32[256]{0:T(256)S(1)}, u32[]{:S(2)}) copy-start(f32[256]{0:T(256)S(1)} %add_rsqrt_fusion.1) | copy-start | bytes 3076
  72.2 11.0 %copy-start.10 = (bf16[256,128]{1,0:T(8,128)(2,1)}, bf16[256,128]{1,0:T(8,128)(2,1)S(1)}, u32[]{:S(2)}) copy-start(bf16[256,128]{1,0:T(8,128)(2,1)S(1)} %convolution_convert_fusion.5) | copy-start | bytes 196612
  72.9 118.2 %collective-permute-start.1 = (bf16[128,128]{1,0:T(8,128)(2,1)}, bf16[128,128]{1,0:T(8,128)(2,1)}, u32[]{:S(2)}, u32[]{:S(2)}) collective-permute-start(bf16[128,128]{1,0:T(8,128)(2,1)} %slice.64), channel_id=1, source_target_pairs={{0,8},{8,16},{16,24},{1,9},{9,17},{17,25},{2,10},{10,18},{18,26},{... | collective-permute-start | bytes 98312 | tf_op jit(solution)/shard_map/ppermute | solution.py:41
  176.6 1.3 copy-start.8
  178.8 7.6 %copy-start.19 = (f32[256]{0:T(256)S(1)}, f32[256]{0:T(256)}, u32[]{:S(2)}) copy-start(f32[256]{0:T(256)} %copy-done.18) | copy-start | bytes 3076
  178.8 7.6 %copy-start.21 = (f32[2048]{0:T(1024)S(1)}, f32[2048]{0:T(1024)}, u32[]{:S(2)}) copy-start(f32[2048]{0:T(1024)} %param.19) | copy-start | bytes 24580
  185.6 2.7 copy-start.11
  186.4 104.1 %all-gather.24.cloned.1.call-start = ((), (), s32[]{:S(2)}) async-start(), calls=%async_computation.9 | async-start | bytes 2621440 | tf_op jit(solution)/shard_map/all_gather | solution.py:209
  188.3 31.2 %copy-start.6 = (bf16[1,256,2048]{2,1,0:T(8,128)(2,1)S(1)}, bf16[1,256,2048]{2,1,0:T(8,128)(2,1)}, u32[]{:S(2)}) copy-start(bf16[1,256,2048]{2,1,0:T(8,128)(2,1)} %all-gather.20.cloned.1.call-done) | copy-start | bytes 3145732
  188.6 4.3 %collective-permute-start = (bf16[128,128]{1,0:T(8,128)(2,1)S(1)}, bf16[128,128]{1,0:T(8,128)(2,1)S(1)}, u32[]{:S(2)}, u32[]{:S(2)}) collective-permute-start(bf16[128,128]{1,0:T(8,128)(2,1)S(1)} %slice.63), channel_id=1, source_target_pairs={{0,8},{8,16},{16,24},{1,9},{9,17},{17,25},{2,10},{10,18},{18,26},{... | collective-permute-start | bytes 98312 | tf_op jit(solution)/shard_map/ppermute | solution.py:41
  194.9 27.2 %copy-start.14 = (pred[2,128,256]{1,2,0:T(8,128)(4,1)S(1)}, pred[2,128,256]{1,2,0:T(8,128)(4,1)}, u32[]{:S(2)}) copy-start(pred[2,128,256]{1,2,0:T(8,128)(4,1)} %broadcast_and_fusion) | copy-start | bytes 196612
  221.8 1.0 copy-start.17
  248.9 4.6 %copy-start.2 = (f32[256,2,128]{2,0,1:T(8,128)S(1)}, f32[256,2,128]{2,0,1:T(8,128)}, u32[]{:S(2)}) copy-start(f32[256,2,128]{2,0,1:T(8,128)} %copy-done.1) | copy-start | bytes 786436
  248.9 4.6 %copy-start.4 = (f32[256,2,128]{2,0,1:T(8,128)S(1)}, f32[256,2,128]{2,0,1:T(8,128)}, u32[]{:S(2)}) copy-start(f32[256,2,128]{2,0,1:T(8,128)} %copy-done.3) | copy-start | bytes 786436
  248.9 4.6 %copy-start.9 = (f32[1,2,256,256]{3,2,1,0:T(8,128)S(1)}, f32[1,2,256,256]{3,2,1,0:T(8,128)}, u32[]{:S(2)}) copy-start(f32[1,2,256,256]{3,2,1,0:T(8,128)} %param.27) | copy-start | bytes 1572868
  253.5 1.3 copy-start.16
  255.9 65.2 %reduce-scatter.2.cloned.1.call-start = ((), (), s32[]{:S(2)}) async-start(), calls=%async_computation.6 | async-start | bytes 1572864 | tf_op jit(solution)/shard_map/reduce_scatter | solution.py:218
  293.3 1.0 copy-start.7
  (2 other events, 1.5 us)
Sparse Core Ops, SparseCore 0:
  8.9 11.7 all-gather.19
  22.3 58.6 all-gather.11
  82.5 45.0 all-gather.15
  129.1 44.4 all-gather.13
  175.0 44.4 all-gather.17
  220.9 27.9 all-gather.21
  256.0 34.4 all-gather.23
  313.2 7.8 reduce-scatter.1
where the time goes:
time: 331 us; the launch traced here: 330 us
  waiting for transfers between devices  188 us (57%)
  blocking collectives  69.8 us (21%)
  matrix products  23 us (7%)
  local copies, waits for them, and re-layouts  16.4 us (5%)
  between operations  14.8 us (4%)
  other arithmetic  12.8 us (4%)
  starting transfers between devices  5.19 us (2%)
    all_gather x1, waiting for transfers between devices, shards(): lax.all_gather(weights[0], 'sp', axis=0, tiled=True)  44 us
    all_gather x1, waiting for transfers between devices, shards(): lax.all_gather(weights[2], 'sp', axis=0, tiled=True)  42.1 us
    all_gather x1, waiting for transfers between devices, shards(): piece = lax.all_gather(joined, 'fs', axis=0, tiled=True)  34.5 us
    all_gather x1, waiting for transfers between devices, carried_in(): lax.all_gather(part.astype(kind), axis)  25.1 us
    all_gather x1, waiting for transfers between devices, shards(): lax.all_gather(weights[3], 'sp', axis=0, tiled=True)  24.5 us
    all_gather x1, blocking collectives, shards(): lax.all_gather(weights[5], 'sp', axis=0, tiled=True)  21.2 us
    all_gather x1, blocking collectives, shards(): lax.all_gather(weights[4], 'sp', axis=0, tiled=True)  18.4 us
    all_to_all x1, blocking collectives, shards(): lax.all_to_all(partial_rows, 'fs', split_axis=0, concat_axis=2, tiled=True)  16.7 us
  transfers between devices with their start and end apart: 10, of which 8 were waited for; matrix products, arithmetic and copies ran while one was open for 11% of the time, Pallas kernels for 0%

commit v1 on v0

--- a/solution.py
+++ b/solution.py
@@ -214,7 +214,19 @@
         "srh,hd->srd", piece[:, :, ret_width:], att_out, preferred_element_type=jnp.float32
     )
     partial_rows = product.astype(jnp.bfloat16)
-    regrouped = lax.all_to_all(partial_rows, "fs", split_axis=0, concat_axis=2, tiled=True)
+    ways, here = (lax.axis_size("fs"), lax.axis_index("fs"))
+    width = partial_rows.shape[0] // ways
+    dims = list(partial_rows.shape)
+    dims[0] = width
+    height = dims[2]
+    dims[2] = height * ways
+    full = jnp.zeros(dims, partial_rows.dtype)
+    for mask in range(ways):
+        part_2 = lax.dynamic_slice_in_dim(partial_rows, (here ^ mask) * width, width, axis=0)
+        if mask:
+            part_2 = lax.ppermute(part_2, "fs", [(d, d ^ mask) for d in range(ways)])
+        full = lax.dynamic_update_slice_in_dim(full, part_2, (here ^ mask) * height, axis=2)
+    regrouped = full
     mixed = lax.psum_scatter(
         regrouped[0].astype(jnp.float32).astype(jnp.bfloat16), "tp", scatter_dimension=1, tiled=True
     )

time: 331 us -> 328 us (level)
  blocking collectives: 69.8 us -> 53 us
  waiting for transfers between devices: 188 us -> 196 us
  starting transfers between devices: 5.19 us -> 8.76 us
    all_to_all x1 -> x0, blocking collectives: 16.7 us -> none  [shards(): lax.all_to_all(partial_rows, 'fs', split_axis=0, concat_axis=2, tiled=True)]
    ppermute x0 -> x3, waiting for transfers between devices: none -> 10.1 us  [shards(): part_2 = lax.ppermute(part_2, 'fs', [(d, d ^ mask) for d in range(ways)])]
    ppermute x0 -> x3, starting transfers between devices: none -> 3.55 us  [shards(): part_2 = lax.ppermute(part_2, 'fs', [(d, d ^ mask) for d in range(ways)])]
  transfers between devices with their start and end apart: 10 -> 13, of which waited for: 8 -> 10; matrix products, arithmetic and copies ran while one was open for 11% -> 12% of each run, Pallas kernels for 0% -> 0%
where the time goes in v1:
time: 328 us; the launch traced here: 327 us
  waiting for transfers between devices  196 us (60%)
  blocking collectives  53 us (16%)
  matrix products  23.8 us (7%)
  local copies, waits for them, and re-layouts  18.1 us (6%)
  between operations  14.8 us (5%)
  other arithmetic  12.2 us (4%)
  starting transfers between devices  8.76 us (3%)
    all_gather x1, waiting for transfers between devices, shards(): lax.all_gather(weights[0], 'sp', axis=0, tiled=True)  44 us
    all_gather x1, waiting for transfers between devices, shards(): lax.all_gather(weights[2], 'sp', axis=0, tiled=True)  42.1 us
    all_gather x1, waiting for transfers between devices, shards(): piece = lax.all_gather(joined, 'fs', axis=0, tiled=True)  34.5 us
    all_gather x1, waiting for transfers between devices, carried_in(): lax.all_gather(part.astype(kind), axis)  24.2 us
    all_gather x1, waiting for transfers between devices, shards(): lax.all_gather(weights[3], 'sp', axis=0, tiled=True)  23.4 us
    all_gather x1, blocking collectives, shards(): lax.all_gather(weights[5], 'sp', axis=0, tiled=True)  21.1 us
    all_gather x1, blocking collectives, shards(): lax.all_gather(weights[4], 'sp', axis=0, tiled=True)  18.3 us
    dot_general x6, matrix products, shards(): jnp.dot(normed, piece, preferred_element_type=jnp.float32)  13.6 us
  transfers between devices with their start and end apart: 13, of which 10 were waited for; matrix products, arithmetic and copies ran while one was open for 12% of the time, Pallas kernels for 0%

profile of v1, /device:TPU:0, one launch (start us, length us, event | category | flops | bytes accessed | tf_op | source)
XLA Modules:
  0.0 327.3 jit_solution(3347074958839519074)
XLA Ops:
  12.8 13.6 %all-reduce = bf16[8]{0:T(256)(128)(2,1)S(1)} all-reduce(bf16[8]{0:T(256)(128)(2,1)S(1)} %dynamic-update-slice), channel_id=3, replica_groups=mesh['sp'=4,'fs'=4,'tp'=2] {'sp'}, use_global_device_ids=true, to_apply=%add | all-reduce | flops 8 | bytes 32
  26.5 18.3 %all_gather.42 = bf16[2048,128]{1,0:T(8,128)(2,1)S(1)} all-gather(bf16[512,128]{1,0:T(8,128)(2,1)S(1)} %copy-done.11), channel_id=1, replica_groups=mesh['sp'=4,'fs'=4,'tp'=2] {'sp'}, dimensions={0}, use_global_device_ids=true | all-gather | bytes 655360 | tf_op jit(solution)/shard_map/all_gather | solution.py:127
  45.6 21.1 %all_gather.41 = bf16[2048,128]{1,0:T(8,128)(2,1)} all-gather(bf16[512,128]{1,0:T(8,128)(2,1)S(1)} %copy-done.12), channel_id=1, replica_groups=mesh['sp'=4,'fs'=4,'tp'=2] {'sp'}, dimensions={0}, use_global_device_ids=true | all-gather | bytes 655360 | tf_op jit(solution)/shard_map/all_gather | solution.py:128
  68.0 1.6 fusion.25
  69.6 1.7 convolution_convert_fusion.5
  72.0 2.7 collective-permute-start.1
  74.7 6.2 %all-gather.12.cloned.1.call-done = bf16[2048,512]{1,0:T(8,128)(2,1)} async-done(((bf16[512,512]{1,0:T(8,128)(2,1)}), bf16[2048,512]{1,0:T(8,128)(2,1)}) %all-gather.12.cloned.1.call-update) | async-done | bytes 2097168 | tf_op jit(solution)/shard_map/all_gather | solution.py:124
  80.8 2.3 fusion.31
  83.5 44.0 %all-gather.16.cloned.1.call-done = bf16[2048,512]{1,0:T(8,128)(2,1)} async-done(((bf16[512,512]{1,0:T(8,128)(2,1)}), bf16[2048,512]{1,0:T(8,128)(2,1)}) %all-gather.16.cloned.1.call-update) | async-done | bytes 2097168 | tf_op jit(solution)/shard_map/all_gather | solution.py:123
  127.5 2.7 fusion.33
  131.4 42.1 %all-gather.14.cloned.1.call-done = bf16[2048,512]{1,0:T(8,128)(2,1)} async-done(((bf16[512,512]{1,0:T(8,128)(2,1)}), bf16[2048,512]{1,0:T(8,128)(2,1)}) %all-gather.14.cloned.1.call-update) | async-done | bytes 2097168 | tf_op jit(solution)/shard_map/all_gather | solution.py:125
  173.5 2.7 fusion.32
  176.5 1.2 fusion.65
  178.7 6.8 %while.29 = (s32[]{:T(128)}, f32[2,256,256]{2,1,0:T(8,128)S(1)}, f32[2,2,128,256]{3,2,1,0:T(8,128)}, f32[2,2,128]{2,1,0:T(2,128)S(1)}, f32[2,2,128,256]{3,2,0,1:...) while((s32[]{:T(128)}, f32[2,256,256]{2,1,0:T(8,128)S(1)}, ...), condition=%wide.region_3.4_spmd.clone, body=%wide.region_1.3_spmd.clone.sunk | while | flops 604880896 | bytes 4242084 | solution.py:148
  180.1 1.2 fusion.95
  183.5 1.2 fusion.95
  186.3 1.9 convolution_convert_fusion.6
  189.1 2.2 collective-permute-start
  194.3 1.3 copy.63
  196.0 23.4 %all-gather.18.cloned.1.call-done = bf16[2048,512]{1,0:T(8,128)(2,1)} async-done(((bf16[512,512]{1,0:T(8,128)(2,1)}), bf16[2048,512]{1,0:T(8,128)(2,1)}) %all-gather.18.cloned.1.call-update) | async-done | bytes 2097168 | tf_op jit(solution)/shard_map/all_gather | solution.py:126
  219.4 2.4 convolution_convert_fusion.1
  222.0 1.5 fusion.29
  224.6 24.2 %all-gather.22.cloned.1.call-done = bf16[8,256,256]{2,1,0:T(8,128)(2,1)} async-done(((bf16[2,256,256]{2,1,0:T(8,128)(2,1)}), bf16[8,256,256]{2,1,0:T(8,128)(2,1)}) %all-gather.22.cloned.1.call-update) | async-done | bytes 1048592 | tf_op jit(solution)/shard_map/all_gather | solution.py:18
  248.8 4.6 %while.30 = (s32[]{:T(128)}, f32[2]{0:T(128)S(1)}, f32[2,256,256]{2,1,0:T(8,128)S(1)}, s32[]{:T(128)}, bf16[4,2]{1,0:T(4,128)(2,1)S(1)}, /*index=5*/bf16[4,2,256,256]{3,2,1,0:T(8,128)(2,1)}, s32[]{:T(128)}, s32[]{:T(128)}) while((s32[]{:T(128)}, f32[2]{0:T(128)S(1)}, f32[2,256,256]{2,1,0:T(8,128)S(1)}, s32[]{:T(128)}, ...), condition=%wide.region_7.8_spmd.clone, body=%wide.region_6.7_spmd.clone.sunk | while | flops 655372 | bytes 1310871 | solution.py:35
  248.8 1.2 fusion.96
  255.9 34.5 %all-gather.24.cloned.1.call-done = bf16[1024,1024]{0,1:T(8,128)(2,1)} async-done(((bf16[256,1024]{0,1:T(8,128)(2,1)}), bf16[1024,1024]{0,1:T(8,128)(2,1)}) %all-gather.24.cloned.1.call-update) | async-done | bytes 2097168 | tf_op jit(solution)/shard_map/all_gather | solution.py:209
  290.4 2.9 copy.79
  296.0 1.5 collective-permute-start.2
  298.1 1.5 collective-permute-start.4
  300.7 4.6 %collective-permute-done.2 = bf16[1,256,512]{2,1,0:T(8,128)(2,1)S(1)} collective-permute-done((bf16[1,256,512]{2,1,0:T(8,128)(2,1)S(1)}, bf16[1,256,512]{2,1,0:T(8,128)(2,1)S(1)}, u32[]{:S(2)}, u32[]{:S(2)}) %collective-permute-start.2) | collective-permute-done | bytes 262176 | tf_op jit(solution)/shard_map/ppermute | solution.py:227
  305.3 5.5 %collective-permute-done.3 = bf16[1,256,512]{2,1,0:T(8,128)(2,1)S(1)} collective-permute-done((bf16[1,256,512]{2,1,0:T(8,128)(2,1)S(1)}, bf16[1,256,512]{2,1,0:T(8,128)(2,1)S(1)}, u32[]{:S(2)}, u32[]{:S(2)}) %collective-permute-start.3) | collective-permute-done | bytes 262176 | tf_op jit(solution)/shard_map/ppermute | solution.py:227
  311.9 8.5 %reduce-scatter.2.cloned.1.call-done = bf16[256,1024]{1,0:T(8,128)(2,1)} async-done(((bf16[256,2048]{1,0:T(8,128)(2,1)}), bf16[256,1024]{1,0:T(8,128)(2,1)}) %reduce-scatter.2.cloned.1.call-update) | async-done | bytes 524304 | tf_op jit(solution)/shard_map/reduce_scatter | solution.py:230
  (163 shorter events, 32.8 us)
Async XLA Ops:
  6.5 286.7 %copy-start = (bf16[512,512]{1,0:T(8,128)(2,1)S(1)}, bf16[512,512]{1,0:T(8,128)(2,1)}, u32[]{:S(2)}) copy-start(bf16[512,512]{1,0:T(8,128)(2,1)} %param.30) | copy-start | bytes 1572868
  6.5 4.8 %copy-start.23 = (u32[32]{0:T(128)S(1)}, u32[32]{0:T(128)}, u32[]{:S(2)}) copy-start(u32[32]{0:T(128)} %constant.115) | copy-start | bytes 388
  6.5 3.5 %copy-start.16 = (f32[1,2,256]{2,1,0:T(2,128)S(1)}, f32[1,2,256]{2,1,0:T(2,128)}, u32[]{:S(2)}) copy-start(f32[1,2,256]{2,1,0:T(2,128)} %param.26) | copy-start | bytes 6148
  6.5 20.0 %copy-start.11 = (bf16[512,128]{1,0:T(8,128)(2,1)S(1)}, bf16[512,128]{1,0:T(8,128)(2,1)}, u32[]{:S(2)}) copy-start(bf16[512,128]{1,0:T(8,128)(2,1)} %param.24) | copy-start | bytes 393220
  6.5 38.4 %copy-start.22 = (f32[8]{0:T(128)S(1)}, f32[8]{0:T(128)}, u32[]{:S(2)}) copy-start(f32[8]{0:T(128)} %param.29) | copy-start | bytes 100
  6.5 39.0 %copy-start.12 = (bf16[512,128]{1,0:T(8,128)(2,1)S(1)}, bf16[512,128]{1,0:T(8,128)(2,1)}, u32[]{:S(2)}) copy-start(bf16[512,128]{1,0:T(8,128)(2,1)} %param.25) | copy-start | bytes 393220
  6.6 61.4 %all-gather.20.cloned.1.call-start = ((), (), s32[]{:S(2)}) async-start(), calls=%async_computation.6 | async-start | bytes 1572864 | tf_op jit(solution)/shard_map/all_gather | solution.py:111
  7.3 73.5 %all-gather.12.cloned.1.call-start = ((), (), s32[]{:S(2)}) async-start(), calls=%async_computation.1 | async-start | bytes 2621440 | tf_op jit(solution)/shard_map/all_gather | solution.py:124
  8.0 61.6 %copy-start.21 = (f32[2048]{0:T(1024)S(1)}, f32[2048]{0:T(1024)}, u32[]{:S(2)}) copy-start(f32[2048]{0:T(1024)} %param.19) | copy-start | bytes 24580
  8.1 119.5 %all-gather.16.cloned.1.call-start = ((), (), s32[]{:S(2)}) async-start(), calls=%async_computation.3 | async-start | bytes 2621440 | tf_op jit(solution)/shard_map/all_gather | solution.py:123
  8.8 164.7 %all-gather.14.cloned.1.call-start = ((), (), s32[]{:S(2)}) async-start(), calls=%async_computation.2 | async-start | bytes 2621440 | tf_op jit(solution)/shard_map/all_gather | solution.py:125
  9.4 210.0 %all-gather.18.cloned.1.call-start = ((), (), s32[]{:S(2)}) async-start(), calls=%async_computation.4 | async-start | bytes 2621440 | tf_op jit(solution)/shard_map/all_gather | solution.py:126
  10.0 238.8 %all-gather.22.cloned.1.call-start = ((), (), s32[]{:S(2)}) async-start(), calls=%async_computation.7 | async-start | bytes 1310720 | tf_op jit(solution)/shard_map/all_gather | solution.py:18
  68.0 12.8 %copy-start.7 = (bf16[1,256,2048]{2,1,0:T(8,128)(2,1)S(1)}, bf16[1,256,2048]{2,1,0:T(8,128)(2,1)}, u32[]{:S(2)}) copy-start(bf16[1,256,2048]{2,1,0:T(8,128)(2,1)} %all-gather.20.cloned.1.call-done) | copy-start | bytes 3145732
  69.6 116.7 %copy-start.19 = (f32[256]{0:T(256)}, f32[256]{0:T(256)S(1)}, u32[]{:S(2)}) copy-start(f32[256]{0:T(256)S(1)} %add_rsqrt_fusion.1) | copy-start | bytes 3076
  72.0 119.5 %collective-permute-start.1 = (bf16[128,128]{1,0:T(8,128)(2,1)}, bf16[128,128]{1,0:T(8,128)(2,1)}, u32[]{:S(2)}, u32[]{:S(2)}) collective-permute-start(bf16[128,128]{1,0:T(8,128)(2,1)} %slice.64), channel_id=1, source_target_pairs={{0,8},{8,16},{16,24},{1,9},{9,17},{17,25},{2,10},{10,18},{18,26},{... | collective-permute-start | bytes 98312 | tf_op jit(solution)/shard_map/ppermute | solution.py:41
  186.3 104.1 %all-gather.24.cloned.1.call-start = ((), (), s32[]{:S(2)}) async-start(), calls=%async_computation.8 | async-start | bytes 2621440 | tf_op jit(solution)/shard_map/all_gather | solution.py:209
  188.2 31.2 %copy-start.8 = (bf16[1,256,2048]{2,1,0:T(8,128)(2,1)S(1)}, bf16[1,256,2048]{2,1,0:T(8,128)(2,1)}, u32[]{:S(2)}) copy-start(bf16[1,256,2048]{2,1,0:T(8,128)(2,1)} %all-gather.20.cloned.1.call-done) | copy-start | bytes 3145732
  189.1 4.3 %collective-permute-start = (bf16[128,128]{1,0:T(8,128)(2,1)S(1)}, bf16[128,128]{1,0:T(8,128)(2,1)S(1)}, u32[]{:S(2)}, u32[]{:S(2)}) collective-permute-start(bf16[128,128]{1,0:T(8,128)(2,1)S(1)} %slice.63), channel_id=1, source_target_pairs={{0,8},{8,16},{16,24},{1,9},{9,17},{17,25},{2,10},{10,18},{18,26},{... | collective-permute-start | bytes 98312 | tf_op jit(solution)/shard_map/ppermute | solution.py:41
  192.3 27.1 %copy-start.20 = (f32[256]{0:T(256)S(1)}, f32[256]{0:T(256)}, u32[]{:S(2)}) copy-start(f32[256]{0:T(256)} %copy-done.19) | copy-start | bytes 3076
  196.0 26.1 %copy-start.13 = (bf16[2,128,2,64]{1,3,2,0:T(8,128)(2,1)S(1)}, bf16[2,128,2,64]{1,3,2,0:T(8,128)(2,1)}, u32[]{:S(2)}) copy-start(bf16[2,128,2,64]{1,3,2,0:T(8,128)(2,1)} %copy.74) | copy-start | bytes 196612
  221.7 1.8 copy-start.18
  221.7 1.9 copy-start.14
  221.7 1.9 copy-start.15
  248.8 4.6 %copy-start.4 = (f32[256,2,128]{2,0,1:T(8,128)S(1)}, f32[256,2,128]{2,0,1:T(8,128)}, u32[]{:S(2)}) copy-start(f32[256,2,128]{2,0,1:T(8,128)} %copy-done.3) | copy-start | bytes 786436
  248.8 4.6 %copy-start.6 = (f32[256,2,128]{2,0,1:T(8,128)S(1)}, f32[256,2,128]{2,0,1:T(8,128)}, u32[]{:S(2)}) copy-start(f32[256,2,128]{2,0,1:T(8,128)} %copy-done.5) | copy-start | bytes 786436
  248.8 4.6 %copy-start.10 = (f32[1,2,256,256]{3,2,1,0:T(8,128)S(1)}, f32[1,2,256,256]{3,2,1,0:T(8,128)}, u32[]{:S(2)}) copy-start(f32[1,2,256,256]{3,2,1,0:T(8,128)} %param.27) | copy-start | bytes 1572868
  253.4 1.3 copy-start.17
  255.8 64.6 %reduce-scatter.2.cloned.1.call-start = ((), (), s32[]{:S(2)}) async-start(), calls=%async_computation.5 | async-start | bytes 1572864 | tf_op jit(solution)/shard_map/reduce_scatter | solution.py:230
  296.0 9.2 %collective-permute-start.2 = (bf16[1,256,512]{2,1,0:T(8,128)(2,1)S(1)}, bf16[1,256,512]{2,1,0:T(8,128)(2,1)S(1)}, u32[]{:S(2)}, u32[]{:S(2)}) collective-permute-start(bf16[1,256,512]{2,1,0:T(8,128)(2,1)S(1)} %get-tuple-element.248), channel_id=1, source_target_pairs={{0,2},{2,0},{4,6},{6,4},{1,3},{3,1},{5,7},{7,5},{8,10},{10,8},{12,... | collective-permute-start | bytes 786440 | tf_op jit(solution)/shard_map/ppermute | solution.py:227
  297.6 13.2 %collective-permute-start.3 = (bf16[1,256,512]{2,1,0:T(8,128)(2,1)S(1)}, bf16[1,256,512]{2,1,0:T(8,128)(2,1)S(1)}, u32[]{:S(2)}, u32[]{:S(2)}) collective-permute-start(bf16[1,256,512]{2,1,0:T(8,128)(2,1)S(1)} %get-tuple-element.247), channel_id=1, source_target_pairs={{0,4},{2,6},{4,0},{6,2},{1,5},{3,7},{5,1},{7,3},{8,12},{10,14},{12... | collective-permute-start | bytes 786440 | tf_op jit(solution)/shard_map/ppermute | solution.py:227
  298.1 12.7 %collective-permute-start.4 = (bf16[1,256,512]{2,1,0:T(8,128)(2,1)S(1)}, bf16[1,256,512]{2,1,0:T(8,128)(2,1)S(1)}, u32[]{:S(2)}, u32[]{:S(2)}) collective-permute-start(bf16[1,256,512]{2,1,0:T(8,128)(2,1)S(1)} %get-tuple-element.246), channel_id=1, source_target_pairs={{0,6},{2,4},{4,2},{6,0},{1,7},{3,5},{5,3},{7,1},{8,14},{10,12},{12... | collective-permute-start | bytes 786440 | tf_op jit(solution)/shard_map/ppermute | solution.py:227
  (5 other events, 4.6 us)
Sparse Core Ops, SparseCore 0:
  8.9 11.7 all-gather.19
  22.3 58.5 all-gather.11
  82.4 45.0 all-gather.15
  129.0 44.4 all-gather.13
  174.9 44.4 all-gather.17
  220.8 27.9 all-gather.21
  255.9 34.4 all-gather.23
  312.0 8.3 reduce-scatter.1
